TPU v7x, 512 devices: a whole 4x4x16 slice. The times are simulated.
512 devices in a mesh: sp: 32 (over z, core), tp: 16 (over y, x).
Axes of the slice: x: 4, y: 4, z: 16, core: 2. Of those that a mesh axis runs over, the one named last changes fastest.
Arguments:
- residual_in: bfloat16 [8192, 2048], P('sp'), may hold values from -3 to 3
- mix_gain: float32 [2048], replicated, may hold values from 0.1 to 1.9
- pool_weight: bfloat16 [512, 2048], P(None, 'tp'), may hold values from -0.5 to 0.5
- pool_scale: float32 [2048], P('tp'), may hold values from 0.1 to 1.9
- ffn_gain: float32 [2048], replicated, may hold values from 0.1 to 1.9
- route_ids: int32 [8192, 2], P('sp'), may hold values from 0 to 31, all different within a row; in each aligned block of 16 rows (0 to 15, 16 to 31, ...) at most 2 rows name the same one
- route_weights: float32 [8192, 2], P('sp'), may hold values from 0.1 to 1
- gate_weight: bfloat16 [32, 2048, 3584], P('sp', None, 'tp'), may hold values from -0.125 to 0.125
- up_weight: bfloat16 [32, 2048, 3584], P('sp', None, 'tp'), may hold values from -0.125 to 0.125
- down_weight: bfloat16 [32, 3584, 2048], P('sp', 'tp'), may hold values from -0.09375 to 0.09375
Outputs:
- layer_out: bfloat16 [8192, 2048], P('sp')
Inputs may be any that keep to these rules, and one draw needn't show every extreme that they name: `route_ids`: each row names 2 different experts; in each aligned block of 16 rows no expert is named by more than 2 rows, and some block has an expert named by exactly 2 rows.
All inputs are finite; a program needn't handle non-finite values.
Results may differ from a plain program's by a relative error of at most 0.0074.
Values may be sent and summed in bfloat16 or wider, within the bound.
No kernel may reach another device: no remote copies, remote signals or barrier semaphores. Data moves between devices by JAX's collectives and lax.ppermute only.
A program may use at most 64 MiB of HBM per device.

v0:
```python
import jax
import jax.numpy as jnp
from jax import lax
from jax.sharding import Mesh
from jax.sharding import PartitionSpec as P

GROUPS = 4
SPAN = 16
TOP_K = 2
SP = ("sp_0", "sp_1")
EPS = 1e-06


def from_behind(value, axis, steps):
    count = lax.axis_size(axis)
    first, last = (max(0, -steps), min(count, count - steps))
    return lax.ppermute(value, axis, [(source, source + steps) for source in range(first, last)])


def split_up(shard, dim, size):
    before, after = (shard.shape[:dim], shard.shape[dim + 1 :])
    return jnp.moveaxis(shard.reshape(*before, size, -1, *after), dim, 0)


def sent_and_summed(shard, axis, dim):
    size = lax.axis_size(axis)
    blocks = lax.all_to_all(split_up(shard, dim, size), axis, 0, 0, tiled=True)
    return jnp.sum(blocks.astype(jnp.float32), axis=0)


def in_order(blocks, dim):
    dims = list(blocks.shape[1:])
    dims[dim] *= blocks.shape[0]
    return jnp.moveaxis(blocks, 0, dim).reshape(dims)


def exchange_in_order(blocks, axes, order):
    dims = [lax.axis_size(a) for a in axes]
    blocks = blocks.reshape(*dims, *blocks.shape[1:])
    for k in order:
        blocks = lax.all_to_all(blocks, axes[k], split_axis=k, concat_axis=k, tiled=True)
    return blocks.reshape(-1, *blocks.shape[len(axes) :])


def core_and_chips(shard, groups, order, split_dim, concat_dim):
    size = lax.axis_size(groups[0]) * lax.axis_size(groups[1])
    blocks = split_up(shard, split_dim, size)
    return in_order(exchange_in_order(blocks, groups, order), concat_dim)


def copy_for_each(shard, axis):
    size = lax.axis_size(axis)
    return lax.all_to_all(
        jnp.broadcast_to(shard[None], (size, *shard.shape)), axis, 0, 0, tiled=True
    )


def gather_directly(shard, axis, dim):
    blocks = copy_for_each(shard, axis)
    return in_order(blocks, dim)


def rms_scale(values, gain):
    return values * lax.rsqrt(jnp.mean(values * values, axis=-1, keepdims=True) + EPS) * gain


def slot_table(chosen_ids, experts, capacity):
    flat_ids = chosen_ids.reshape(-1)
    matches = (flat_ids[:, None] == jnp.arange(experts, dtype=jnp.int32)[None, :]).astype(jnp.int32)
    before = jnp.cumsum(matches, axis=0) - matches
    slot_of = jnp.sum(before * matches, axis=1)
    target = flat_ids * capacity + slot_of
    return (target[:, None] == jnp.arange(experts * capacity, dtype=jnp.int32)[None, :]).astype(
        jnp.float32
    )


def shards(
    residual_in,
    mix_gain,
    pool_weight,
    pool_scale,
    ffn_gain,
    route_ids,
    route_weights,
    gate_weight,
    up_weight,
    down_weight,
):
    tp_count = lax.axis_size("tp")
    sp_count = lax.axis_size(SP)
    tp_index = lax.axis_index("tp")
    tok_count, width = residual_in.shape
    group_width = width // GROUPS
    col_count = pool_weight.shape[1]
    row_count = tok_count // tp_count
    capacity = 2 * TOP_K * row_count // sp_count
    group_index = tp_index * col_count // group_width
    window = jnp.power(2, group_index + 1)
    stream = residual_in.astype(jnp.float32)
    inverse = lax.rsqrt(jnp.mean(stream * stream, axis=-1, keepdims=True) + EPS)
    stream_group = lax.dynamic_slice_in_dim(stream, group_index * group_width, group_width, 1)
    gain_group = lax.dynamic_slice_in_dim(mix_gain, group_index * group_width, group_width, 0)
    normed_group = (stream_group * inverse * gain_group).astype(jnp.bfloat16)
    rim_rows = from_behind(normed_group[tok_count - SPAN :], SP, 1)
    extended = jnp.concatenate([rim_rows, normed_group], axis=0).astype(jnp.float32)
    window_sum = jnp.zeros((tok_count, group_width), jnp.float32)
    for offset in range(SPAN):
        window_sum = window_sum + jnp.where(
            offset < window, extended[SPAN - offset : SPAN - offset + tok_count], 0.0
        )
    position = lax.axis_index(SP) * tok_count + jnp.arange(tok_count, dtype=jnp.int32)
    divisor = jnp.minimum(position + 1, window).astype(jnp.float32)
    pooled = (window_sum / divisor[:, None] - extended[SPAN:]).astype(jnp.bfloat16)
    mixed = (jnp.dot(pooled, pool_weight, preferred_element_type=jnp.float32) * pool_scale).astype(
        jnp.bfloat16
    )
    stream_own = lax.dynamic_slice_in_dim(stream, tp_index * row_count, row_count, 0)
    mixed_own = lax.all_to_all(mixed, "tp", split_axis=0, concat_axis=1, tiled=True)
    after_own = (stream_own + mixed_own.astype(jnp.float32)).astype(jnp.bfloat16)
    normed_own = rms_scale(after_own.astype(jnp.float32), ffn_gain).astype(jnp.bfloat16)
    ids_own = lax.dynamic_slice_in_dim(route_ids, tp_index * row_count, row_count, 0)
    table_own = slot_table(ids_own, sp_count, capacity)
    repeated = jnp.repeat(normed_own, TOP_K, axis=0)
    outgoing = lax.dot_general(
        table_own.astype(jnp.bfloat16),
        repeated,
        (((0,), (0,)), ((), ())),
        preferred_element_type=jnp.float32,
    )
    outgoing = outgoing.astype(jnp.bfloat16).reshape(sp_count, capacity, width)
    arrived = lax.all_to_all(outgoing, SP, split_axis=0, concat_axis=0, tiled=True)
    piece = lax.all_gather(arrived, "tp", axis=0, tiled=True)
    flat_rows = piece.reshape(-1, width)
    gate_part = jnp.dot(flat_rows, gate_weight[0], preferred_element_type=jnp.float32)
    up_part = jnp.dot(flat_rows, up_weight[0], preferred_element_type=jnp.float32)
    hidden = (jax.nn.silu(gate_part) * up_part).astype(jnp.bfloat16)
    hidden_all = hidden.reshape(piece.shape[0], piece.shape[1], hidden.shape[1])
    hidden_flat = hidden_all.reshape(-1, hidden_all.shape[-1])
    term = jnp.dot(hidden_flat, down_weight[0], preferred_element_type=jnp.float32)
    summed = sent_and_summed(
        term.astype(jnp.bfloat16).astype(jnp.float32).astype(jnp.bfloat16), "tp", 0
    )
    expert_out = summed.astype(jnp.bfloat16).reshape(sp_count, capacity, width)
    returned_rows = core_and_chips(expert_out, ("sp_0", "sp_1"), (1, 0), 0, 0)
    weights_own = lax.dynamic_slice_in_dim(route_weights, tp_index * row_count, row_count, 0)
    weight_table = jnp.einsum(
        "rk,rkc->rc", weights_own, table_own.reshape(row_count, TOP_K, sp_count * capacity)
    )
    expert_mix = jnp.dot(
        weight_table,
        returned_rows.reshape(-1, width).astype(jnp.float32),
        precision=lax.Precision.HIGHEST,
    )
    out_own = (after_own.astype(jnp.float32) + expert_mix).astype(jnp.bfloat16)
    return gather_directly(out_own, "tp", 0)


def solution(mesh):
    torus = Mesh(mesh.devices.reshape(16, 2, mesh.shape["tp"]), ("sp_0", "sp_1", "tp"))
    return jax.shard_map(
        shards,
        mesh=torus,
        in_specs=(
            P(SP, None),
            P(),
            P(None, "tp"),
            P("tp"),
            P(),
            P(SP, None),
            P(SP, None),
            P(SP, None, "tp"),
            P(SP, None, "tp"),
            P(SP, "tp", None),
        ),
        out_specs=P(SP, None),
        check_vma=False,
    )
```

profile of v0, /device:TPU:32, one launch (start us, length us, event | category | flops | bytes accessed | tf_op | source)
XLA Modules:
  0.0 268.7 jit_solution(1426922073096499499)
XLA Ops:
  6.5 1.6 multiply_reduce_fusion
  8.1 1.5 convert_element_type.67
  9.6 0.8 dynamic_slice.17
  10.4 0.1 multiply_convert_fusion
  10.5 1.9 collective-permute-start
  12.5 0.1 constant_dynamic-slice_fusion
  12.6 0.1 copy.24
  12.7 0.1 eq.35
  12.8 0.1 fusion.40
  12.8 0.1 reduce_window_sum.11
  12.9 0.2 select_reduce_fusion
  13.1 2.5 collective-permute-done
  15.6 0.1 maximum_convert_fusion
  15.7 0.0 copy-start.1
  15.7 2.0 fusion.2
  17.7 7.0 %all-to-all-start = ((bf16[16,16,128]{2,1,0:T(8,128)(2,1)}), bf16[16,16,128]{2,1,0:T(8,128)(2,1)S(1)}, u32[]{:S(2)}, u32[]{:S(2)}) async-start(bf16[16,16,128]{2,1,0:T(8,128)(2,1)} %bitcast), calls=%async_computation | async-start | bytes 131072 | tf_op jit(solution)/shard_map/all_to_all | solution.py:119
  24.8 0.0 all-gather.2.cloned.1.call-start
  24.8 7.6 %all-to-all-done = bf16[16,16,128]{2,1,0:T(8,128)(2,1)S(1)} async-done(((bf16[16,16,128]{2,1,0:T(8,128)(2,1)}), bf16[16,16,128]{2,1,0:T(8,128)(2,1)S(1)}, u32[]{:S(2)}, u32[]{:S(2)}) %all-to-all-start) | async-done | bytes 65568 | tf_op jit(solution)/shard_map/all_to_all | solution.py:119
  32.4 0.1 fusion.33
  32.6 0.1 fusion.35
  32.7 0.1 broadcast_in_dim.38
  32.8 0.1 reshape.67
  32.8 0.3 convolution_convert_fusion.1
  33.2 0.2 reshape.68
  33.3 37.4 %all_to_all.38 = bf16[32,2,2048]{2,1,0:T(2,128)(2,1)} all-to-all(bf16[32,2,2048]{2,1,0:T(2,128)(2,1)S(1)} %reshape.68), channel_id=1, replica_groups=mesh['sp_0'=16,'sp_1'=2,'tp'=16] {'sp_0','sp_1'}, dimensions={0} | all-to-all | bytes 524288 | tf_op jit(solution)/shard_map/all_to_all | solution.py:132
  70.8 0.0 all-gather.2.cloned.1.call-update
  70.8 0.0 copy-start.3
  70.8 56.0 %all-gather.2.cloned.1.call-done = bf16[512,2,2048]{2,1,0:T(2,128)(2,1)} async-done(((bf16[32,2,2048]{2,1,0:T(2,128)(2,1)}), bf16[512,2,2048]{2,1,0:T(2,128)(2,1)}) %all-gather.2.cloned.1.call-update) | async-done | bytes 4194320 | tf_op jit(solution)/shard_map/all_gather | solution.py:133
  126.8 7.2 %reshape.69 = bf16[1024,2048]{1,0:T(8,128)(2,1)} reshape(bf16[512,2,2048]{2,1,0:T(2,128)(2,1)} %all-gather.2.cloned.1.call-done) | data formatting | bytes 8388608 | tf_op jit(solution)/shard_map/reshape | solution.py:134
  134.0 4.6 %fusion.6 = f32[1024,224]{0,1:T(8,128)} fusion(bf16[1024,2048]{1,0:T(8,128)(2,1)} %reshape.69, bf16[1,2048,224]{1,2,0:T(8,128)(2,1)S(1)} %copy-done.3), kind=kOutput, calls=%fused_computation.11 | convolution fusion | flops 939524096 | bytes 6029312 | tf_op jit(solution)/shard_map/dot_general | solution.py:135
  138.6 7.0 %convolution_convert_fusion = bf16[1024,2048]{1,0:T(8,128)(2,1)} fusion(bf16[1024,2048]{1,0:T(8,128)(2,1)} %reshape.69, bf16[1,224,2048]{2,1,0:T(8,128)(2,1)S(1)} %copy-done, bf16[1,2048,224]{1,2,0:T(8,128)(2,1)S(1)} %copy-done.4, f32[1024,224]{0,1:T(8,128)} %fusion.6), kind=kOutput, calls=%fused_computation | convolution fusion | flops 1882521600 | bytes 11141120 | tf_op jit(solution)/shard_map/dot_general | solution.py:140
  145.6 56.0 %all_to_all.39 = bf16[16,64,2048]{2,1,0:T(8,128)(2,1)} all-to-all(bf16[16,64,2048]{2,1,0:T(8,128)(2,1)} %bitcast.35), channel_id=1, replica_groups=mesh['sp_0'=16,'sp_1'=2,'tp'=16] {'tp'}, dimensions={0} | all-to-all | bytes 8388608 | tf_op jit(solution)/shard_map/all_to_all | solution.py:27
  201.7 3.0 %reduce_sum.45 = bf16[64,2048]{1,0:T(8,128)(2,1)S(1)} reduce(bf16[16,64,2048]{2,1,0:T(8,128)(2,1)} %all_to_all.39, bf16[]{:T(256)} %constant.97.clone.1), dimensions={0}, to_apply=%region_4.5 | reduce | flops 1966080 | bytes 4456450 | tf_op jit(solution)/shard_map/reduce_sum | solution.py:28
  204.6 0.2 reshape_reshape_reshape.6
  204.8 0.2 copy.20
  205.0 3.9 %all_to_all.40 = bf16[16,2,1,2,2048]{4,3,0,2,1:T(2,128)(2,1)S(1)} all-to-all(bf16[16,2,1,2,2048]{4,3,0,2,1:T(2,128)(2,1)S(1)} %copy.20), channel_id=1, replica_groups=mesh['sp_0'=16,'sp_1'=2,'tp'=16] {'sp_1'}, dimensions={1} | all-to-all | bytes 524288 | tf_op jit(solution)/shard_map/all_to_all | solution.py:41
  209.0 1.0 copy.21
  209.9 12.7 %all-to-all-start.4 = ((bf16[16,2,1,2,2048]{4,3,1,2,0:T(2,128)(2,1)}), bf16[16,2,1,2,2048]{4,3,1,2,0:T(2,128)(2,1)S(1)}, u32[]{:S(2)}, u32[]{:S(2)}) async-start(bf16[16,2,1,2,2048]{4,3,1,2,0:T(2,128)(2,1)} %copy.21), calls=%async_computation.4 | async-start | bytes 524288 | tf_op jit(solution)/shard_map/all_to_all | solution.py:41
  222.6 0.1 reduce_sum.43
  222.7 0.8 dynamic-slice_bitcast_fusion
  223.4 0.1 copy.22
  223.5 0.2 fusion.37
  223.7 17.2 %all-to-all-done.4 = bf16[16,2,1,2,2048]{4,3,1,2,0:T(2,128)(2,1)S(1)} async-done(((bf16[16,2,1,2,2048]{4,3,1,2,0:T(2,128)(2,1)}), bf16[16,2,1,2,2048]{4,3,1,2,0:T(2,128)(2,1)S(1)}, u32[]{:S(2)}, u32[]{:S(2)}) %all-to-all-start.4) | async-done | bytes 262176 | tf_op jit(solution)/shard_map/all_to_all | solution.py:41
  241.0 0.1 reshape_reshape_reshape.7
  241.1 0.2 fusion
  241.3 0.1 broadcast_in_dim.39
  241.4 19.5 %all_to_all.41 = bf16[16,16,2048]{2,1,0:T(8,128)(2,1)S(1)} all-to-all(bf16[16,16,2048]{2,1,0:T(8,128)(2,1)S(1)} %broadcast_in_dim.39), channel_id=1, replica_groups=mesh['sp_0'=16,'sp_1'=2,'tp'=16] {'tp'}, dimensions={0} | all-to-all | bytes 2097152 | tf_op jit(solution)/shard_map/all_to_all | solution.py:53
  260.9 1.0 copy.29
  (18 shorter events, 0.1 us)
Async XLA Ops:
  6.5 132.1 %copy-start = (bf16[1,224,2048]{2,1,0:T(8,128)(2,1)S(1)}, bf16[1,224,2048]{2,1,0:T(8,128)(2,1)}, u32[]{:S(2)}) copy-start(bf16[1,224,2048]{2,1,0:T(8,128)(2,1)} %param.19) | copy-start | bytes 2752516
  6.5 6.0 %copy-start.2 = (s32[256,2]{0,1:T(2,128)S(1)}, s32[256,2]{0,1:T(2,128)}, u32[]{:S(2)}) copy-start(s32[256,2]{0,1:T(2,128)} %param.15) | copy-start | bytes 6148
  6.5 9.1 %copy-start.6 = (f32[128]{0:T(128)S(1)}, f32[128]{0:T(128)}, u32[]{:S(2)}) copy-start(f32[128]{0:T(128)} %param.13) | copy-start | bytes 1540
  6.5 9.1 %copy-start.5 = (bf16[512,128]{1,0:T(8,128)(2,1)S(1)}, bf16[512,128]{1,0:T(8,128)(2,1)}, u32[]{:S(2)}) copy-start(bf16[512,128]{1,0:T(8,128)(2,1)} %param.12) | copy-start | bytes 393220
  10.5 5.1 %collective-permute-start = (bf16[16,512]{1,0:T(8,128)(2,1)S(1)}, bf16[16,512]{1,0:T(8,128)(2,1)S(1)}, u32[]{:S(2)}, u32[]{:S(2)}) collective-permute-start(bf16[16,512]{1,0:T(8,128)(2,1)S(1)} %slice.69), channel_id=1, source_target_pairs={{0,16},{16,32},{32,48},{48,64},{64,80},{80,96},{96,112},{112,128},... | collective-permute-start | bytes 49160 | tf_op jit(solution)/shard_map/ppermute | solution.py:17
  15.7 16.9 %copy-start.1 = (f32[2048]{0:T(1024)S(1)}, f32[2048]{0:T(1024)}, u32[]{:S(2)}) copy-start(f32[2048]{0:T(1024)} %param.14) | copy-start | bytes 24580
  17.7 14.7 %all-to-all-start = ((bf16[16,16,128]{2,1,0:T(8,128)(2,1)}), bf16[16,16,128]{2,1,0:T(8,128)(2,1)S(1)}, u32[]{:S(2)}, u32[]{:S(2)}) async-start(bf16[16,16,128]{2,1,0:T(8,128)(2,1)} %bitcast), calls=%async_computation | async-start | bytes 131072 | tf_op jit(solution)/shard_map/all_to_all | solution.py:119
  24.8 102.0 %all-gather.2.cloned.1.call-start = ((), (), s32[]{:S(2)}) async-start(), calls=%async_computation.6 | async-start | bytes 4456448 | tf_op jit(solution)/shard_map/all_gather | solution.py:133
  70.8 63.2 %copy-start.3 = (bf16[1,2048,224]{1,2,0:T(8,128)(2,1)S(1)}, bf16[1,2048,224]{1,2,0:T(8,128)(2,1)}, u32[]{:S(2)}) copy-start(bf16[1,2048,224]{1,2,0:T(8,128)(2,1)} %param.17) | copy-start | bytes 2752516
  134.0 4.6 %copy-start.4 = (bf16[1,2048,224]{1,2,0:T(8,128)(2,1)S(1)}, bf16[1,2048,224]{1,2,0:T(8,128)(2,1)}, u32[]{:S(2)}) copy-start(bf16[1,2048,224]{1,2,0:T(8,128)(2,1)} %param.18) | copy-start | bytes 2752516
  209.9 31.0 %all-to-all-start.4 = ((bf16[16,2,1,2,2048]{4,3,1,2,0:T(2,128)(2,1)}), bf16[16,2,1,2,2048]{4,3,1,2,0:T(2,128)(2,1)S(1)}, u32[]{:S(2)}, u32[]{:S(2)}) async-start(bf16[16,2,1,2,2048]{4,3,1,2,0:T(2,128)(2,1)} %copy.21), calls=%async_computation.4 | async-start | bytes 524288 | tf_op jit(solution)/shard_map/all_to_all | solution.py:41
Sparse Core Ops, SparseCore 0:
  70.9 55.8 all-gather.1
where the time goes:
time: 269 us
  blocking collectives  117 us (43%)
  waiting for transfers between devices  83.3 us (31%)
  starting transfers between devices  21.7 us (8%)
  matrix products  14.4 us (5%)
  between operations  13.7 us (5%)
  local copies, waits for them, and re-layouts  12 us (4%)
  other arithmetic  6.75 us (3%)
    all_to_all x1, blocking collectives, sent_and_summed(): blocks = lax.all_to_all(split_up(shard, dim, size), axis, 0, 0, tiled=True)  56 us
    all_gather x1, waiting for transfers between devices, shards(): piece = lax.all_gather(arrived, 'tp', axis=0, tiled=True)  56 us
    all_to_all x1, blocking collectives, shards(): lax.all_to_all(outgoing, SP, split_axis=0, concat_axis=0, tiled=True)  37.4 us
    all_to_all x1, blocking collectives, copy_for_each(): lax.all_to_all(jnp.broadcast_to(shard[None], (size, *shard.shape)), axis,...  19.5 us
    all_to_all x1, waiting for transfers between devices, exchange_in_order(): lax.all_to_all(blocks, axes[k], split_axis=k, concat_axis=k, tiled=True)  17.2 us
    all_to_all x1, starting transfers between devices, exchange_in_order(): lax.all_to_all(blocks, axes[k], split_axis=k, concat_axis=k, tiled=True)  12.7 us
    all_to_all x1, waiting for transfers between devices, shards(): lax.all_to_all(mixed, 'tp', split_axis=0, concat_axis=1, tiled=True)  7.6 us
    reshape x1, local copies, waits for them, and re-layouts, shards(): flat_rows = piece.reshape(-1, width)  7.21 us
  transfers between devices with their start and end apart: 4, of which 4 were waited for; matrix products, arithmetic and copies ran while one was open for 1% of the time, Pallas kernels for 0%

commit v1 on v0

--- a/solution.py
+++ b/solution.py
@@ -9,6 +9,12 @@
 TOP_K = 2
 SP = ("sp_0", "sp_1")
 EPS = 1e-06
+
+
+def _handle_quarters(m):
+    return jnp.concatenate(
+        lax.all_to_all(jnp.stack(lax.axis_size("tp") * [m], axis=0), "tp", 0, 0), axis=0
+    )
 
 
 def from_behind(value, axis, steps):
@@ -130,7 +136,7 @@
     )
     outgoing = outgoing.astype(jnp.bfloat16).reshape(sp_count, capacity, width)
     arrived = lax.all_to_all(outgoing, SP, split_axis=0, concat_axis=0, tiled=True)
-    piece = lax.all_gather(arrived, "tp", axis=0, tiled=True)
+    piece = _handle_quarters(arrived)
     flat_rows = piece.reshape(-1, width)
     gate_part = jnp.dot(flat_rows, gate_weight[0], preferred_element_type=jnp.float32)
     up_part = jnp.dot(flat_rows, up_weight[0], preferred_element_type=jnp.float32)

time: 269 us -> 251 us (0.933)
  waiting for transfers between devices: 83.3 us -> 27.3 us
  blocking collectives: 117 us -> 170 us
  between operations: 13.7 us -> 0.34 us
  starting transfers between devices: 21.7 us -> 15.8 us
  local copies, waits for them, and re-layouts: 12 us -> 15.3 us
    all_gather x1 -> x0, waiting for transfers between devices: 56 us -> none  [shards(): piece = lax.all_gather(arrived, 'tp', axis=0, tiled=True)]
    all_to_all x0 -> x1, blocking collectives: none -> 53.8 us  [_handle_quarters(): lax.all_to_all(jnp.stack(lax.axis_size('tp') * [m], axis=0), 'tp', 0, 0)]
    another operation x0 -> x2, local copies, waits for them, and re-layouts: none -> 10.5 us  [the longest x1 7.29 us: shards(): flat_rows = piece.reshape(-1, width)]
    reshape x1 -> x0, local copies, waits for them, and re-layouts: 7.21 us -> none  [shards(): flat_rows = piece.reshape(-1, width)]
    all_to_all x1, starting transfers between devices: 12.7 us -> 6.8 us  [exchange_in_order(): lax.all_to_all(blocks, axes[k], split_axis=k, concat_axis=k, tiled=True)]
  transfers between devices with their start and end apart: 4 -> 3, of which waited for: 4 -> 3; matrix products, arithmetic and copies ran while one was open for 1% -> 1% of each run, Pallas kernels for 0% -> 0%
where the time goes in v1:
time: 251 us; the launch traced here: 250 us
  blocking collectives  170 us (68%)
  waiting for transfers between devices  27.3 us (11%)
  starting transfers between devices  15.8 us (6%)
  local copies, waits for them, and re-layouts  15.3 us (6%)
  matrix products  14.4 us (6%)
  other arithmetic  6.75 us (3%)
    all_to_all x1, blocking collectives, sent_and_summed(): blocks = lax.all_to_all(split_up(shard, dim, size), axis, 0, 0, tiled=True)  55.4 us
    all_to_all x1, blocking collectives, _handle_quarters(): lax.all_to_all(jnp.stack(lax.axis_size('tp') * [m], axis=0), 'tp', 0, 0)  53.8 us
    all_to_all x1, blocking collectives, shards(): lax.all_to_all(outgoing, SP, split_axis=0, concat_axis=0, tiled=True)  37.3 us
    all_to_all x1, blocking collectives, copy_for_each(): lax.all_to_all(jnp.broadcast_to(shard[None], (size, *shard.shape)), axis,...  19.4 us
    all_to_all x1, waiting for transfers between devices, exchange_in_order(): lax.all_to_all(blocks, axes[k], split_axis=k, concat_axis=k, tiled=True)  17.2 us
    all_to_all x1, waiting for transfers between devices, shards(): lax.all_to_all(mixed, 'tp', split_axis=0, concat_axis=1, tiled=True)  7.65 us
    another operation x1, local copies, waits for them, and re-layouts, shards(): flat_rows = piece.reshape(-1, width)  7.29 us
    all_to_all x1, starting transfers between devices, shards(): lax.all_to_all(mixed, 'tp', split_axis=0, concat_axis=1, tiled=True)  7.03 us
  transfers between devices with their start and end apart: 3, of which 3 were waited for; matrix products, arithmetic and copies ran while one was open for 1% of the time, Pallas kernels for 0%

profile of v1, /device:TPU:32, one launch (start us, length us, event | category | flops | bytes accessed | tf_op | source)
XLA Modules:
  0.0 249.8 jit_solution(1737925058649027134)
XLA Ops:
  0.0 1.6 multiply_reduce_fusion
  1.6 1.5 convert_element_type.67
  3.1 0.8 dynamic_slice.17
  3.9 0.1 multiply_convert_fusion
  4.0 1.9 collective-permute-start
  6.0 0.1 constant_dynamic-slice_fusion
  6.1 0.1 copy.24
  6.2 0.1 eq.35
  6.2 0.1 fusion.40
  6.3 0.1 reduce_window_sum.11
  6.4 0.2 select_reduce_fusion
  6.6 2.5 collective-permute-done
  9.1 0.1 maximum_convert_fusion
  9.1 0.0 copy-done.6
  9.1 0.0 copy-done.5
  9.2 0.0 copy-start.1
  9.2 2.0 fusion.2
  11.2 7.0 %all-to-all-start = ((bf16[16,16,128]{2,1,0:T(8,128)(2,1)}), bf16[16,16,128]{2,1,0:T(8,128)(2,1)S(1)}, u32[]{:S(2)}, u32[]{:S(2)}) async-start(bf16[16,16,128]{2,1,0:T(8,128)(2,1)} %bitcast), calls=%async_computation | async-start | bytes 131072 | tf_op jit(solution)/shard_map/all_to_all | solution.py:125
  18.3 7.7 %all-to-all-done = bf16[16,16,128]{2,1,0:T(8,128)(2,1)S(1)} async-done(((bf16[16,16,128]{2,1,0:T(8,128)(2,1)}), bf16[16,16,128]{2,1,0:T(8,128)(2,1)S(1)}, u32[]{:S(2)}, u32[]{:S(2)}) %all-to-all-start) | async-done | bytes 65568 | tf_op jit(solution)/shard_map/all_to_all | solution.py:125
  25.9 0.1 fusion.33
  26.1 0.1 fusion.35
  26.2 0.1 broadcast_in_dim.38
  26.2 0.1 reshape.66
  26.3 0.3 convolution_convert_fusion.1
  26.6 0.2 reshape.67
  26.8 37.3 %all_to_all.43 = bf16[32,2,2048]{2,1,0:T(2,128)(2,1)S(1)} all-to-all(bf16[32,2,2048]{2,1,0:T(2,128)(2,1)S(1)} %reshape.67), channel_id=1, replica_groups=mesh['sp_0'=16,'sp_1'=2,'tp'=16] {'sp_0','sp_1'}, dimensions={0} | all-to-all | bytes 524288 | tf_op jit(solution)/shard_map/all_to_all | solution.py:138
  64.2 3.2 %stack.2 = bf16[16,32,2,2048]{3,2,1,0:T(2,128)(2,1)S(1)} broadcast(bf16[32,2,2048]{2,1,0:T(2,128)(2,1)S(1)} %all_to_all.43), dimensions={1,2,3} | broadcast | bytes 4456448 | tf_op jit(solution)/shard_map/stack | solution.py:16
  67.4 53.8 %all_to_all.44 = bf16[16,32,2,2048]{3,2,1,0:T(2,128)(2,1)} all-to-all(bf16[16,32,2,2048]{3,2,1,0:T(2,128)(2,1)S(1)} %stack.2), channel_id=1, replica_groups=mesh['sp_0'=16,'sp_1'=2,'tp'=16] {'tp'}, dimensions={0} | all-to-all | bytes 8388608 | tf_op jit(solution)/shard_map/all_to_all | solution.py:16
  121.2 7.3 %reshape_reshape.3 = bf16[1024,2048]{1,0:T(8,128)(2,1)} reshape(bf16[16,32,2,2048]{3,2,1,0:T(2,128)(2,1)} %all_to_all.44) | data formatting | bytes 8388608 | tf_op jit(solution)/shard_map/reshape;reshape | solution.py:140
  128.5 4.6 %fusion.6 = f32[1024,224]{0,1:T(8,128)} fusion(bf16[1024,2048]{1,0:T(8,128)(2,1)} %reshape_reshape.3, bf16[1,2048,224]{1,2,0:T(8,128)(2,1)S(1)} %copy-done.3), kind=kOutput, calls=%fused_computation.11 | convolution fusion | flops 939524096 | bytes 6029312 | tf_op jit(solution)/shard_map/dot_general | solution.py:141
  133.1 7.0 %convolution_convert_fusion = bf16[1024,2048]{1,0:T(8,128)(2,1)} fusion(bf16[1024,2048]{1,0:T(8,128)(2,1)} %reshape_reshape.3, bf16[1,224,2048]{2,1,0:T(8,128)(2,1)S(1)} %copy-done, bf16[1,2048,224]{1,2,0:T(8,128)(2,1)S(1)} %copy-done.4, f32[1024,224]{0,1:T(8,128)} %fusion.6), kind=kOutput, calls=%fused_computation | convolution fusion | flops 1882521600 | bytes 11141120 | tf_op jit(solution)/shard_map/dot_general | solution.py:146
  140.2 55.4 %all_to_all.45 = bf16[16,64,2048]{2,1,0:T(8,128)(2,1)} all-to-all(bf16[16,64,2048]{2,1,0:T(8,128)(2,1)} %bitcast.35), channel_id=1, replica_groups=mesh['sp_0'=16,'sp_1'=2,'tp'=16] {'tp'}, dimensions={0} | all-to-all | bytes 8388608 | tf_op jit(solution)/shard_map/all_to_all | solution.py:33
  195.5 3.0 %reduce_sum.45 = bf16[64,2048]{1,0:T(8,128)(2,1)S(1)} reduce(bf16[16,64,2048]{2,1,0:T(8,128)(2,1)} %all_to_all.45, bf16[]{:T(256)} %constant.97.clone.1), dimensions={0}, to_apply=%region_4.5 | reduce | flops 1966080 | bytes 4456450 | tf_op jit(solution)/shard_map/reduce_sum | solution.py:34
  198.5 0.2 reshape_reshape_reshape.6
  198.7 0.2 copy.20
  198.9 3.9 %all_to_all.46 = bf16[16,2,1,2,2048]{4,3,0,2,1:T(2,128)(2,1)S(1)} all-to-all(bf16[16,2,1,2,2048]{4,3,0,2,1:T(2,128)(2,1)S(1)} %copy.20), channel_id=1, replica_groups=mesh['sp_0'=16,'sp_1'=2,'tp'=16] {'sp_1'}, dimensions={1} | all-to-all | bytes 524288 | tf_op jit(solution)/shard_map/all_to_all | solution.py:47
  202.8 1.0 copy.21
  203.8 6.8 %all-to-all-start.5 = ((bf16[16,2,1,2,2048]{4,3,1,2,0:T(2,128)(2,1)}), bf16[16,2,1,2,2048]{4,3,1,2,0:T(2,128)(2,1)S(1)}, u32[]{:S(2)}, u32[]{:S(2)}) async-start(bf16[16,2,1,2,2048]{4,3,1,2,0:T(2,128)(2,1)} %copy.21), calls=%async_computation.5 | async-start | bytes 524288 | tf_op jit(solution)/shard_map/all_to_all | solution.py:47
  210.6 0.1 reduce_sum.43
  210.7 0.8 dynamic-slice_bitcast_fusion
  211.4 0.1 copy.22
  211.6 0.2 fusion.37
  211.8 17.2 %all-to-all-done.5 = bf16[16,2,1,2,2048]{4,3,1,2,0:T(2,128)(2,1)S(1)} async-done(((bf16[16,2,1,2,2048]{4,3,1,2,0:T(2,128)(2,1)}), bf16[16,2,1,2,2048]{4,3,1,2,0:T(2,128)(2,1)S(1)}, u32[]{:S(2)}, u32[]{:S(2)}) %all-to-all-start.5) | async-done | bytes 262176 | tf_op jit(solution)/shard_map/all_to_all | solution.py:47
  229.0 0.1 reshape_reshape_reshape.7
  229.1 0.2 fusion
  229.3 0.1 broadcast_in_dim.39
  229.4 19.4 %all_to_all.47 = bf16[16,16,2048]{2,1,0:T(8,128)(2,1)S(1)} all-to-all(bf16[16,16,2048]{2,1,0:T(8,128)(2,1)S(1)} %broadcast_in_dim.39), channel_id=1, replica_groups=mesh['sp_0'=16,'sp_1'=2,'tp'=16] {'tp'}, dimensions={0} | all-to-all | bytes 2097152 | tf_op jit(solution)/shard_map/all_to_all | solution.py:59
  248.8 1.0 copy.29
  (17 shorter events, 0.1 us)
Async XLA Ops:
  0.0 133.1 %copy-start = (bf16[1,224,2048]{2,1,0:T(8,128)(2,1)S(1)}, bf16[1,224,2048]{2,1,0:T(8,128)(2,1)}, u32[]{:S(2)}) copy-start(bf16[1,224,2048]{2,1,0:T(8,128)(2,1)} %param.19) | copy-start | bytes 2752516
  0.0 6.0 %copy-start.2 = (s32[256,2]{0,1:T(2,128)S(1)}, s32[256,2]{0,1:T(2,128)}, u32[]{:S(2)}) copy-start(s32[256,2]{0,1:T(2,128)} %param.15) | copy-start | bytes 6148
  0.0 9.1 %copy-start.6 = (f32[128]{0:T(128)S(1)}, f32[128]{0:T(128)}, u32[]{:S(2)}) copy-start(f32[128]{0:T(128)} %param.13) | copy-start | bytes 1540
  0.0 9.1 %copy-start.5 = (bf16[512,128]{1,0:T(8,128)(2,1)S(1)}, bf16[512,128]{1,0:T(8,128)(2,1)}, u32[]{:S(2)}) copy-start(bf16[512,128]{1,0:T(8,128)(2,1)} %param.12) | copy-start | bytes 393220
  4.0 5.1 %collective-permute-start = (bf16[16,512]{1,0:T(8,128)(2,1)S(1)}, bf16[16,512]{1,0:T(8,128)(2,1)S(1)}, u32[]{:S(2)}, u32[]{:S(2)}) collective-permute-start(bf16[16,512]{1,0:T(8,128)(2,1)S(1)} %slice.69), channel_id=1, source_target_pairs={{0,16},{16,32},{32,48},{48,64},{64,80},{80,96},{96,112},{112,128},... | collective-permute-start | bytes 49160 | tf_op jit(solution)/shard_map/ppermute | solution.py:23
  9.2 16.9 %copy-start.1 = (f32[2048]{0:T(1024)S(1)}, f32[2048]{0:T(1024)}, u32[]{:S(2)}) copy-start(f32[2048]{0:T(1024)} %param.14) | copy-start | bytes 24580
  11.2 14.7 %all-to-all-start = ((bf16[16,16,128]{2,1,0:T(8,128)(2,1)}), bf16[16,16,128]{2,1,0:T(8,128)(2,1)S(1)}, u32[]{:S(2)}, u32[]{:S(2)}) async-start(bf16[16,16,128]{2,1,0:T(8,128)(2,1)} %bitcast), calls=%async_computation | async-start | bytes 131072 | tf_op jit(solution)/shard_map/all_to_all | solution.py:125
  121.2 7.3 %copy-start.3 = (bf16[1,2048,224]{1,2,0:T(8,128)(2,1)S(1)}, bf16[1,2048,224]{1,2,0:T(8,128)(2,1)}, u32[]{:S(2)}) copy-start(bf16[1,2048,224]{1,2,0:T(8,128)(2,1)} %param.17) | copy-start | bytes 2752516
  128.5 4.6 %copy-start.4 = (bf16[1,2048,224]{1,2,0:T(8,128)(2,1)S(1)}, bf16[1,2048,224]{1,2,0:T(8,128)(2,1)}, u32[]{:S(2)}) copy-start(bf16[1,2048,224]{1,2,0:T(8,128)(2,1)} %param.18) | copy-start | bytes 2752516
  203.8 25.2 %all-to-all-start.5 = ((bf16[16,2,1,2,2048]{4,3,1,2,0:T(2,128)(2,1)}), bf16[16,2,1,2,2048]{4,3,1,2,0:T(2,128)(2,1)S(1)}, u32[]{:S(2)}, u32[]{:S(2)}) async-start(bf16[16,2,1,2,2048]{4,3,1,2,0:T(2,128)(2,1)} %copy.21), calls=%async_computation.5 | async-start | bytes 524288 | tf_op jit(solution)/shard_map/all_to_all | solution.py:47
